TPU v7x, 32 devices: a whole 2x2x4 slice. The times are simulated.
32 devices in a mesh: grp: 2 (over y), fs: 4 (over z), tp: 4 (over x, core).
Axes of the slice: x: 2, y: 2, z: 4, core: 2. Of those that a mesh axis runs over, the one named last changes fastest.
Arguments:
- tokens: bfloat16 [8192, 2048], P(('grp', 'fs'), 'tp'), parts along dimension 0, may hold values from -6 to 6
- norm1_gain: float32 [2048], replicated, may hold values from 0.1 to 1.9
- weight_u: float32 [2048, 1024], P('fs', 'tp'), may hold values from -0.125 to 0.125
- weight_v: float32 [2048, 1024], P('fs', 'tp'), may hold values from -0.125 to 0.125
- scale_u: float32 [1024], P('tp'), may hold values from 0.5 to 2
- scale_v: float32 [1024], P('tp'), may hold values from 0.05 to 4.5
- mix_gain: float32 [1024], P('tp'), may hold values from 0.1 to 1.9
- spatial_weight: float32 [4, 128, 128], replicated, may hold values from -0.5 to 0.5
- spatial_bias: float32 [4, 128], replicated, may hold values from 0.5 to 1.5
- weight_out: float32 [1024, 2048], P('tp', 'fs'), may hold values from -0.1875 to 0.1875
- scale_out: float32 [2048], P('fs'), may hold values from 0.5 to 2
- norm2_gain: float32 [2048], replicated, may hold values from 0.1 to 1.9
- weight_up: float32 [2048, 8192], P('fs', 'tp'), may hold values from -0.125 to 0.125
- scale_up: float32 [8192], P('tp'), may hold values from 0.5 to 2
- weight_down: float32 [8192, 2048], P('tp', 'fs'), may hold values from -0.0625 to 0.0625
- scale_down: float32 [2048], P('fs'), may hold values from 0.5 to 2
Outputs:
- result: bfloat16 [8192, 2048], P(('grp', 'fs'), 'tp'), parts along dimension 0
There are 2 independent parts, one for each index of `grp`. A program takes and returns all parts, laid end to end along the dimension named above; an argument that names none is the same for every part. Nothing has to cross between parts.
All inputs are finite; a program needn't handle non-finite values.
Results may differ from a plain program's by a relative error of at most 0.023.
Values may be sent and summed in bfloat16 or wider, within the bound.
A program may use at most 128 MiB of HBM per device.

v0:
```python
import jax
import jax.numpy as jnp
from jax import lax
from jax.experimental import pallas as pl
from jax.experimental.pallas import tpu as pltpu
from jax.sharding import PartitionSpec as P

GM_W = 1024
GROUPS = 4
BLOCK = 128


def swap(value, axis, size, mask):
    return lax.ppermute(value, axis, [(k, k ^ mask) for k in range(size)])


def over_fs(piece, fs, relay, near_too):
    if fs != 4 or not relay:
        return [piece] + [swap(piece, "fs", fs, mask) for mask in range(1, fs)]
    far = swap(piece, "fs", 4, 2)
    near = swap(piece, "fs", 4, 1) if near_too else None
    middle = lax.ppermute(piece, "fs", [(1, 2), (2, 1)])
    relayed = lax.ppermute(far, "fs", [(1, 0), (2, 3)])
    me = lax.axis_index("fs")
    last = jnp.where((me == 1) | (me == 2), middle, relayed)
    return [piece, near, far, last]


def gather_weight(shard, cut_axis, fs, relay=False, whole_near=False):
    half = shard.shape[cut_axis] // 2
    group = lax.axis_index("grp")
    mine = lax.dynamic_slice_in_dim(shard, group * half, half, cut_axis)
    other = lax.dynamic_slice_in_dim(shard, (1 - group) * half, half, cut_axis)
    whole_near = whole_near and relay and fs == 4
    firsts = over_fs(mine, fs, relay, not whole_near)
    if whole_near:
        near = swap(jnp.concatenate([mine, other], axis=cut_axis), "fs", fs, 1)
        firsts[1], near_other = jnp.split(near, 2, axis=cut_axis)
    seconds = [other] + [
        near_other
        if whole_near and mask == 1
        else lax.ppermute(firsts[mask], "grp", [(0, 1), (1, 0)])
        for mask in range(1, fs)
    ]
    return firsts, seconds


def halves_swapped(value, axis):
    half = value.shape[axis] // 2
    group = lax.axis_index("grp")
    return jnp.concatenate(
        [
            lax.dynamic_slice_in_dim(value, group * half, half, axis),
            lax.dynamic_slice_in_dim(value, (1 - group) * half, half, axis),
        ],
        axis=axis,
    )


def gather_rows(piece, tp):
    blocks = [None] * tp
    blocks[0] = piece
    bit = tp // 2
    while bit:
        for at in range(tp):
            if blocks[at] is not None and not at & bit and blocks[at | bit] is None:
                blocks[at | bit] = "due"
        for at in range(tp):
            if isinstance(blocks[at], str):
                blocks[at] = swap(blocks[at ^ bit], "tp", tp, bit)
        bit //= 2
    return blocks


def normed_blocks(blocks, gain, fs, tp):
    feature_count = gain.shape[0]
    width, fine = feature_count // tp, feature_count // fs
    squares = sum(
        jnp.sum(jnp.square(block.astype(jnp.float32)), axis=1) for block in blocks
    )
    inverse = lax.rsqrt(squares / feature_count + 1e-06)[:, None]
    stacked = jnp.stack(blocks)
    me_fs, me_tp = lax.axis_index("fs"), lax.axis_index("tp")
    pieces = []
    for mask in range(fs):
        block = me_fs ^ mask
        first = block * fine
        whole = lax.dynamic_index_in_dim(stacked, (first // width) ^ me_tp, 0, keepdims=False)
        if fine != width:
            whole = lax.dynamic_slice_in_dim(whole, first % width, fine, 1)
        gain_piece = lax.dynamic_slice_in_dim(gain, first, fine, 0)
        pieces.append((whole.astype(jnp.float32) * inverse * gain_piece).astype(jnp.bfloat16))
    return jnp.concatenate(pieces, axis=1)


def scatter_sum(terms, fs, tp):
    stacked = jnp.stack(terms)
    ratio = fs // tp
    me_fs, me_tp = lax.axis_index("fs"), lax.axis_index("tp")
    sums = []
    for mask in range(tp):
        parts = [
            lax.dynamic_index_in_dim(
                stacked, ((me_tp ^ mask) * ratio + at) ^ me_fs, 0, keepdims=False
            )
            for at in range(ratio)
        ]
        sums.append(parts[0] if ratio == 1 else jnp.concatenate(parts, axis=1))
    bit = 1
    while bit < tp:
        kept = {}
        for at in range(tp):
            if sums[at] is not None and not at & bit:
                got = swap(sums[at | bit].astype(jnp.bfloat16), "tp", tp, bit)
                kept[at] = sums[at].astype(jnp.float32) + got.astype(jnp.float32)
        sums = [kept.get(at) for at in range(tp)]
        bit *= 2
    return sums[0]


def make(fs, tp):
    def layer(
        tokens,
        norm1_gain,
        weight_u,
        weight_v,
        scale_u,
        scale_v,
        mix_gain,
        spatial_weight,
        spatial_bias,
        weight_out,
        scale_out,
        norm2_gain,
        weight_up,
        scale_up,
        weight_down,
        scale_down,
    ):
        half = weight_u.shape[1] // 2
        token_blocks = gather_rows(tokens, tp)
        both = jnp.stack([weight_u, weight_v], axis=1).astype(jnp.bfloat16)
        both_mine, both_other = gather_weight(both, 2, fs)
        scales = jnp.stack([scale_out, scale_down])
        all_scales = [scales] + [swap(scales, "fs", fs, mask) for mask in range(1, fs)]
        out_mine, out_other = gather_weight(weight_out.astype(jnp.bfloat16), 0, fs)
        up_mine, up_other = gather_weight(weight_up.astype(jnp.bfloat16), 1, fs, relay=True)
        down_mine, down_other = gather_weight(weight_down.astype(jnp.bfloat16), 0, fs, relay=True, whole_near=True)

        normed_in = normed_blocks(token_blocks, norm1_gain, fs, tp)
        full_u = jnp.concatenate(
            [jnp.concatenate([a[:, 0], b[:, 0]], axis=1) for a, b in zip(both_mine, both_other)]
        )
        full_v = jnp.concatenate(
            [jnp.concatenate([a[:, 1], b[:, 1]], axis=1) for a, b in zip(both_mine, both_other)]
        )
        pre_v = jnp.dot(normed_in, full_v, preferred_element_type=jnp.float32)
        pre_u = jnp.dot(normed_in, full_u, preferred_element_type=jnp.float32)
        act_v = jax.nn.gelu(pre_v * halves_swapped(scale_v, 0))
        gate_u = jax.nn.gelu(pre_u * halves_swapped(scale_u, 0))
        local_width = 2 * half
        row_sums, row_squares = lax.psum(
            (jnp.sum(act_v, axis=1), jnp.sum(act_v * act_v, axis=1)), "tp"
        )
        row_mean = (row_sums / GM_W)[:, None]
        square = (row_squares / GM_W)[:, None]
        v_norm = (
            (act_v - row_mean)
            * lax.rsqrt(square - row_mean * row_mean + 1e-06)
            * halves_swapped(mix_gain, 0)
        ).astype(jnp.bfloat16)
        group_index = lax.axis_index("tp") * local_width // (GM_W // GROUPS)
        lower_mask = jnp.tril(jnp.ones((BLOCK, BLOCK), jnp.float32))
        spatial_mask = (
            lax.dynamic_index_in_dim(spatial_weight, group_index, 0, keepdims=False) * lower_mask
        ).astype(jnp.bfloat16)
        block_bias = lax.dynamic_index_in_dim(spatial_bias, group_index, 0, keepdims=False)
        blocks = v_norm.reshape(-1, BLOCK, local_width)
        mixed = jnp.einsum("ts,nsc->ntc", spatial_mask, blocks, preferred_element_type=jnp.float32)
        mixed = mixed + block_bias[None, :, None]
        gated = (gate_u * mixed.reshape(-1, local_width)).astype(jnp.bfloat16)

        terms = []
        for a, b, scale in zip(out_mine, out_other, all_scales):
            product = jnp.dot(gated, jnp.concatenate([a, b]), preferred_element_type=jnp.float32)
            terms.append((product * scale[0]).astype(jnp.bfloat16))
        mixer_sum = scatter_sum(terms, fs, tp)
        residual = (tokens.astype(jnp.float32) + mixer_sum).astype(jnp.bfloat16)

        normed_mid = normed_blocks(gather_rows(residual, tp), norm2_gain, fs, tp)
        full_up = jnp.concatenate(
            [jnp.concatenate([a, b], axis=1) for a, b in zip(up_mine, up_other)]
        )
        pre_up = jnp.dot(normed_mid, full_up, preferred_element_type=jnp.float32)
        hidden = jnp.square(jax.nn.relu(pre_up * halves_swapped(scale_up, 0))).astype(jnp.bfloat16)
        terms = []
        for a, b, scale in zip(down_mine, down_other, all_scales):
            product = jnp.dot(hidden, jnp.concatenate([a, b]), preferred_element_type=jnp.float32)
            terms.append((product * scale[1]).astype(jnp.bfloat16))
        channel_sum = scatter_sum(terms, fs, tp)
        return (residual.astype(jnp.float32) + channel_sum).astype(jnp.bfloat16)

    return layer


MESH = pl.DeviceIdType.MESH
WAVES = 6
CHUNKS = 4
STEP = 64


def rows_of(first, size, unit):
    return pl.ds(pl.multiple_of(first, unit), size)


def row_loop(first, count, step, body):
    def at(i, carry):
        body(rows_of(first + i * step, step, step))
        return carry

    lax.fori_loop(0, count // step, at, 0)


def matmul(a, b):
    return jnp.dot(a, b, preferred_element_type=jnp.float32)


def fused_kernel(
    tokens, weight_u, weight_v, weight_out, weight_up, weight_down,
    gain1, scale_u, scale_v, mix_gain, spatial_weight, spatial_bias,
    scale_out, scale_down, gain2, scale_up,
    result,
    stage, g_both, g_out, g_up, g_down, tok, mid, normed, hidden,
    act_v, gate_u, gated, stat, stat_rows, scales, terms, core_in, x_out, x_in,
    load_sem, zs, zr, ys, yr, gs, gr, cs, cr, xs, xr, cs2, cr2, xs2, xr2,
    sts, strv, scs, scr,
):
    y, z, t = lax.axis_index("grp"), lax.axis_index("fs"), lax.axis_index("tp")
    other_y = 1 - y
    upper = z // 2
    planes = (z, 1 - z + 4 * upper, 2 - upper, 3 - 3 * upper)
    is_mid = (z == 1) | (z == 2)
    t1 = t + 1 - 2 * (t % 2)
    t2 = (t + 2) % 4
    t3 = (t1 + 2) % 4
    rows, fine = tokens.shape
    chunk = rows // CHUNKS
    width = weight_u.shape[1]
    hid = weight_up.shape[1]
    hhalf = hid // 2
    feature_count = gain1.shape[1]
    sends = []

    def remote(source, target, send, recv, **where):
        return pltpu.make_async_remote_copy(
            src_ref=source, dst_ref=target, send_sem=send, recv_sem=recv,
            device_id=where, device_id_type=MESH,
        )

    barrier = pltpu.get_barrier_semaphore()
    for p in planes[1:]:
        pl.semaphore_signal(barrier, inc=1, device_id={"fs": p}, device_id_type=MESH)
    pl.semaphore_signal(barrier, inc=1, device_id={"grp": other_y}, device_id_type=MESH)
    for u in (t1, t2, t3):
        pl.semaphore_signal(barrier, inc=1, device_id={"tp": u}, device_id_type=MESH)

    def load(source, slot, part=None):
        target = stage.at[slot] if part is None else part
        return pltpu.make_async_copy(source, target, load_sem.at[slot])

    half_w = width
    load_u = load(weight_u, 0, stage.at[0, :, pl.ds(0, half_w)])
    load_v = pltpu.make_async_copy(weight_v, stage.at[0, :, pl.ds(half_w, half_w)], load_sem.at[4])
    load_out = load(weight_out, 1, stage.at[1, pl.ds(0, width), :])
    load_tok = pltpu.make_async_copy(tokens, tok.at[t], load_sem.at[5])

    def load_up(j, slot):
        return load(weight_up.at[:, pl.ds(j * fine, fine)], slot)

    def load_down(j, slot):
        return load(weight_down.at[pl.ds(j * fine, fine), :], slot)

    load_u.start()
    load_v.start()
    load_out.start()
    load_up(0, 2).start()
    load_up(1, 3).start()
    load_tok.start()
    scales[z] = jnp.concatenate([scale_out[...], scale_down[...]], axis=0)

    pl.semaphore_wait(barrier, 7)

    def gather_copies(which, buffer, own_source, r):
        part = pl.ds(r * chunk, chunk)
        to_x = remote(own_source.at[part], buffer.at[t, part], gs.at[which, 0, r], gr.at[which, t, r], tp=t2)
        to_core = remote(own_source.at[part], buffer.at[t, part], gs.at[which, 1, r], gr.at[which, t, r], tp=t1)
        return to_x, to_core

    def gather_start(which, buffer, own_source, r):
        for copy in gather_copies(which, buffer, own_source, r):
            copy.start()
            sends.append(copy)

    def gather_await(which, buffer, block, r):
        part = pl.ds(r * chunk, chunk)
        remote(buffer.at[block, part], buffer.at[block, part], gs.at[which, 2, r], gr.at[which, block, r], tp=t1).wait_recv()

    def gather_relay(which, buffer, r):
        gather_await(which, buffer, t2, r)
        part = pl.ds(r * chunk, chunk)
        copy = remote(buffer.at[t2, part], buffer.at[t2, part], gs.at[which, 2, r], gr.at[which, t2, r], tp=t1)
        copy.start()
        sends.append(copy)

    def piece(w, p, h):
        if w == 0:
            size = fine // 2
            return g_both.at[rows_of(p * fine + h * size, size, size), :]
        if w == 1:
            size = width // 2
            return g_out.at[p, rows_of(h * size, size, size), :]
        if w < 4:
            size = fine // 2
            return g_up.at[h, rows_of(p * fine + (w - 2) * size, size, size), :]
        size = hhalf // 2
        return g_down.at[p, rows_of(h * hhalf + (w - 4) * size, size, size), :]

    def z_copy(w, p, to, slot):
        return remote(piece(w, p, y), piece(w, p, y), zs.at[w, slot], zr.at[w, p], fs=to)

    def y_copy(w, i, h):
        p = planes[i]
        return remote(piece(w, p, h), piece(w, p, h), ys.at[w, i - 1], yr.at[w, p], grp=other_y)

    def own(w):
        z_copy(w, z, planes[1], 0).start()

        @pl.when(is_mid)
        def _():
            z_copy(w, z, planes[2], 1).start()

    def arrive(w, i):
        p = planes[i]
        z_copy(w, p, planes[1], 1 + i).wait_recv()

        @pl.when(is_mid)
        def _():
            z_copy(w, p, planes[2] if i == 1 else planes[1], 1 + i).start()

        y_copy(w, i, y).start()

    def arrive_y(w, i):
        y_copy(w, i, other_y).wait_recv()

    def arrive_all_y(w):
        for i in (1, 2, 3):
            arrive_y(w, i)

    for r in range(CHUNKS):
        gather_start(0, tok, tokens, r)

    def cast_to(slot, count, store):
        row_loop(0, count, STEP, lambda part: store(part, stage[slot, part, :].astype(jnp.bfloat16)))

    def at_offset(part, base):
        return rows_of(part.start + base, part.size, part.size)

    load_u.wait()
    load_v.wait()

    def store_both(part, value):
        g_both[at_offset(part, z * fine), :] = value

    cast_to(0, fine, store_both)
    load_up(2, 0).start()
    load_out.wait()

    def store_out(part, value):
        g_out[z, part, :] = value

    own(0)
    cast_to(1, width, store_out)
    load_up(3, 1).start()
    for i in (1, 2, 3):
        copy = remote(scales.at[z], scales.at[z], scs.at[i - 1], scr.at[z], fs=planes[i])
        copy.start()
        sends.append(copy)

    def cast_up(j, slot):
        load_up(j, slot).wait()
        cols = pl.ds((j % 2) * fine, fine)

        def store(part, value):
            g_up[j // 2, at_offset(part, z * fine), cols] = value

        cast_to(slot, fine, store)

    def cast_down(j, slot):
        load_down(j, slot).wait()

        def store(part, value):
            g_down[z, at_offset(part, j * fine), :] = value

        cast_to(slot, fine, store)

    own(1)
    cast_up(0, 2)
    load_down(0, 2).start()
    gather_relay(0, tok, 0)
    cast_up(1, 3)
    load_down(1, 3).start()
    arrive(0, 1)
    cast_up(2, 0)
    load_down(2, 0).start()
    cast_up(3, 1)
    load_down(3, 1).start()
    arrive(1, 1)
    gather_relay(0, tok, 1)
    arrive(0, 2)
    arrive(1, 2)
    own(2)
    cast_down(0, 2)
    cast_down(1, 3)
    gather_relay(0, tok, 2)
    cast_down(2, 0)
    cast_down(3, 1)
    arrive(0, 3)
    arrive(1, 3)
    own(3)
    load_tok.wait()

    def norm_rows(buffer, gain, first, count):
        def body(part):
            total = jnp.zeros((part.size, 1), jnp.float32)
            for b in range(4):
                value = buffer[b, part, :].astype(jnp.float32)
                total = total + jnp.sum(value * value, axis=1, keepdims=True)
            inverse = lax.rsqrt(total / feature_count + 1e-06)
            for b in range(4):
                value = buffer[b, part, :].astype(jnp.float32)
                cols = pl.ds(b * fine, fine)
                normed[part, cols] = (value * inverse * gain[:, cols]).astype(jnp.bfloat16)

        row_loop(first, count, 32, body)

    def norm_chunk(which, buffer, gain, r):
        gather_await(which, buffer, t1, r)
        gather_await(which, buffer, t3, r)
        norm_rows(buffer, gain, r * chunk, chunk)

    for r in range(CHUNKS):
        if r == CHUNKS - 1:
            gather_relay(0, tok, r)
        norm_chunk(0, tok, gain1, r)

    arrive(2, 1)
    arrive_all_y(0)

    lane = lax.broadcasted_iota(jnp.int32, (chunk, 128), 1)

    def v_chunk(part):
        value = jax.nn.gelu(matmul(normed[part, :], g_both[:, width:]) * scale_v[...])
        act_v[part, :] = value
        total = jnp.sum(value, axis=1, keepdims=True)
        square = jnp.sum(value * value, axis=1, keepdims=True)
        stat[part, :] = jnp.where(lane == 0, total, jnp.where(lane == 1, square, 0.0))

    row_loop(0, rows, chunk, v_chunk)
    stat_rows[0] = stat[...].T[0:8]

    def stat_copy(k, u):
        return remote(stat_rows.at[0], stat_rows.at[k], sts.at[k - 1], strv.at[k], tp=u)

    def u_chunk(part):
        gate_u[part, :] = jax.nn.gelu(matmul(normed[part, :], g_both[:, :width]) * scale_u[...])

    for k, u in ((1, t1), (2, t2), (3, t3)):
        copy = stat_copy(k, u)
        copy.start()
        sends.append(copy)
    row_loop(0, rows, chunk, u_chunk)
    arrive(2, 2)
    for k, u in ((1, t1), (2, t2), (3, t3)):
        stat_copy(k, u).wait_recv()
    totals = stat_rows[0] + stat_rows[1] + stat_rows[2] + stat_rows[3]
    stat[...] = jnp.concatenate([totals, jnp.zeros((120, rows), jnp.float32)], axis=0).T

    down_at = lax.broadcasted_iota(jnp.int32, (BLOCK, BLOCK), 0)
    along = lax.broadcasted_iota(jnp.int32, (BLOCK, BLOCK), 1)
    mask = jnp.where(along <= down_at, spatial_weight[t], 0.0).astype(jnp.bfloat16)
    bias_row = spatial_bias[pl.ds(t, 1), :]
    bias = jnp.sum(jnp.where(along == down_at, bias_row, 0.0), axis=1, keepdims=True)

    def mix_block(part):
        mean = stat[part, 0:1] / GM_W
        square = stat[part, 1:2] / GM_W
        v_norm = (act_v[part, :] - mean) * lax.rsqrt(square - mean * mean + 1e-06) * mix_gain[...]
        mixed = matmul(mask, v_norm.astype(jnp.bfloat16)) + bias
        gated[part, :] = (gate_u[part, :] * mixed).astype(jnp.bfloat16)

    row_loop(0, rows, BLOCK, mix_block)
    arrive_all_y(1)
    for i in (1, 2, 3):
        remote(scales.at[planes[i]], scales.at[planes[i]], scs.at[i - 1], scr.at[planes[i]], fs=planes[i]).wait_recv()

    def core_copy(k, block, r):
        part = pl.ds(r * chunk, chunk)
        return remote(terms.at[block, part], core_in.at[k, part], cs.at[k, r], cr.at[k, r], tp=t1)

    def x_copy(send, recv, r):
        part = pl.ds(r * chunk, chunk)
        return remote(x_out.at[part], x_in.at[part], send.at[r], recv.at[r], tp=t2)

    mix_sends = []
    for r in range(CHUNKS):
        part = pl.ds(r * chunk, chunk)
        for j in range(4):
            product = matmul(gated[part, :], g_out[j])
            terms[j, part, :] = (product * scales[j, 0:1, :]).astype(jnp.bfloat16)
        for k, block in ((0, t1), (1, t3)):
            copy = core_copy(k, block, r)
            copy.start()
            mix_sends.append(copy)

    def pair_out(block, slot, r):
        def body(part):
            both = terms[block, part, :].astype(jnp.float32) + core_in[slot, part, :].astype(jnp.float32)
            x_out[part, :] = both.astype(jnp.bfloat16)

        row_loop(r * chunk, chunk, STEP, body)

    for r in range(CHUNKS):
        core_copy(0, t1, r).wait_recv()
        core_copy(1, t3, r).wait_recv()
        pair_out(t2, 1, r)
        copy = x_copy(xs, xr, r)
        copy.start()
        mix_sends.append(copy)
    own(4)
    arrive(2, 3)

    for r in range(CHUNKS):
        x_copy(xs, xr, r).wait_recv()

        def residual_rows(part):
            total = terms[t, part, :].astype(jnp.float32) + core_in[0, part, :].astype(jnp.float32)
            total = total + x_in[part, :].astype(jnp.float32)
            mid[t, part, :] = (tok[t, part, :].astype(jnp.float32) + total).astype(jnp.bfloat16)

        row_loop(r * chunk, chunk, STEP, residual_rows)
        gather_start(1, mid, mid.at[t], r)
        if r == 1:
            arrive(3, 1)
    arrive(3, 2)
    for copy in mix_sends:
        copy.wait_send()
    own(5)
    for r in range(CHUNKS):
        gather_relay(1, mid, r)
        if r == 2:
            arrive(3, 3)
        if r > 0:
            norm_chunk(1, mid, gain2, r - 1)
    norm_chunk(1, mid, gain2, CHUNKS - 1)

    tile = min(hhalf, fine)

    def up_half(h):
        def body(part):
            for n in range(hhalf // tile):
                cols = pl.ds(n * tile, tile)
                place = rows_of(h * hhalf + n * tile, tile, 128)
                value = matmul(normed[part, :], g_up[h, :, cols]) * scale_up[:, place]
                value = jnp.maximum(value, 0.0)
                hidden[part, place] = (value * value).astype(jnp.bfloat16)

        row_loop(0, rows, chunk, body)

    arrive(4, 1)
    up_half(y)
    arrive(4, 2)
    arrive_all_y(2)
    arrive_all_y(3)
    up_half(other_y)
    arrive(4, 3)

    def chan_core(i, r):
        j = planes[i]
        part = rows_of(r * chunk, chunk, chunk)
        return remote(terms.at[j, part], core_in.at[j // 2, part], cs2.at[i, r], cr2.at[j // 2, r], tp=t1)

    def down_piece(i):
        j = planes[i]
        mine = (j % 2) == (t % 2)

        def one(r, carry):
            part = rows_of(r * chunk, chunk, chunk)
            product = matmul(hidden[part, :], g_down[j])
            terms[j, part, :] = (product * scales[j, 1:2, :]).astype(jnp.bfloat16)

            @pl.when(jnp.logical_not(mine))
            def _():
                chan_core(i, r).start()

            return carry

        lax.fori_loop(0, CHUNKS, one, 0)

        @pl.when(mine)
        def _():
            for r in range(CHUNKS):
                chan_core(i, r).wait_recv()

                @pl.when(j != t)
                def _():
                    pair_out(j, j // 2, r)
                    x_copy(xs2, xr2, r).start()

    down_piece(0)
    arrive(5, 1)
    arrive_y(4, 1)
    arrive(5, 2)
    arrive_y(5, 1)
    down_piece(1)
    arrive(5, 3)
    arrive_y(4, 2)
    arrive_y(5, 2)
    down_piece(2)
    arrive_y(4, 3)
    arrive_y(5, 3)
    down_piece(3)

    for r in range(CHUNKS):
        x_copy(xs2, xr2, r).wait_recv()

        def result_rows(part):
            total = terms[t, part, :].astype(jnp.float32) + core_in[t // 2, part, :].astype(jnp.float32)
            total = total + x_in[part, :].astype(jnp.float32)
            result[part, :] = (mid[t, part, :].astype(jnp.float32) + total).astype(jnp.bfloat16)

        row_loop(r * chunk, chunk, STEP, result_rows)

    for copy in sends:
        copy.wait_send()
    for w in range(WAVES):
        z_copy(w, z, planes[1], 0).wait_send()
        for i in (1, 2, 3):
            y_copy(w, i, y).wait_send()
    for r in range(CHUNKS):
        x_copy(xs2, xr2, r).wait_send()
    for i in range(4):
        @pl.when((planes[i] % 2) != (t % 2))
        def _():
            for r in range(CHUNKS):
                chan_core(i, r).wait_send()

    @pl.when(is_mid)
    def _():
        for w in range(WAVES):
            z_copy(w, z, planes[2], 1).wait_send()
            for i in (1, 2, 3):
                z_copy(w, planes[i], planes[1], 1 + i).wait_send()


def fused_layer(
    tokens, norm1_gain, weight_u, weight_v, scale_u, scale_v, mix_gain, spatial_weight,
    spatial_bias, weight_out, scale_out, norm2_gain, weight_up, scale_up, weight_down, scale_down,
):
    rows, fine = tokens.shape
    depth, width, hid = norm1_gain.shape[0], weight_u.shape[1], weight_up.shape[1]
    bf16, f32 = jnp.bfloat16, jnp.float32
    vmem = lambda shape, kind: pltpu.VMEM(shape, kind)
    dma = lambda *shape: pltpu.SemaphoreType.DMA(shape)
    row = lambda value: value[None, :]
    hbm = pl.BlockSpec(memory_space=pl.ANY)
    local = pl.BlockSpec(memory_space=pltpu.VMEM)
    return pl.pallas_call(
        fused_kernel,
        name="fused_layer",
        out_shape=jax.ShapeDtypeStruct((rows, fine), bf16),
        in_specs=[hbm] * 6 + [local] * 10,
        out_specs=local,
        scratch_shapes=[
            vmem((4, fine, fine), f32),
            vmem((depth, 2 * width), bf16),
            vmem((4, width, fine), bf16),
            vmem((2, depth, hid // 2), bf16),
            vmem((4, hid, fine), bf16),
            vmem((4, rows, fine), bf16),
            vmem((4, rows, fine), bf16),
            vmem((rows, depth), bf16),
            vmem((rows, hid), bf16),
            vmem((rows, width), f32),
            vmem((rows, width), f32),
            vmem((rows, width), bf16),
            vmem((rows, 128), f32),
            vmem((4, 8, rows), f32),
            vmem((4, 2, fine), f32),
            vmem((4, rows, fine), bf16),
            vmem((2, rows, fine), bf16),
            vmem((rows, fine), bf16),
            vmem((rows, fine), bf16),
            dma(6),
            dma(WAVES, 5), dma(WAVES, 4), dma(WAVES, 3), dma(WAVES, 4),
            dma(2, 3, CHUNKS), dma(2, 4, CHUNKS),
            dma(2, CHUNKS), dma(2, CHUNKS), dma(CHUNKS), dma(CHUNKS),
            dma(4, CHUNKS), dma(2, CHUNKS), dma(CHUNKS), dma(CHUNKS),
            dma(3), dma(4), dma(3), dma(4),
        ],
        compiler_params=pltpu.CompilerParams(
            collective_id=0, has_side_effects=True, vmem_limit_bytes=67043328
        ),
    )(
        tokens, weight_u, weight_v, weight_out, weight_up, weight_down,
        row(norm1_gain), row(scale_u), row(scale_v), row(mix_gain), spatial_weight, spatial_bias,
        row(scale_out), row(scale_down), row(norm2_gain), row(scale_up),
    )


def solution(mesh):
    placed = (
        P(("grp", "fs"), "tp"),
        P(),
        P("fs", "tp"),
        P("fs", "tp"),
        P("tp"),
        P("tp"),
        P("tp"),
        P(),
        P(),
        P("tp", "fs"),
        P("fs"),
        P(),
        P("fs", "tp"),
        P("tp"),
        P("tp", "fs"),
        P("fs"),
    )
    grp, fs, tp = mesh.shape["grp"], mesh.shape["fs"], mesh.shape["tp"]
    fused = grp == 2 and fs == 4 and tp == 4
    return jax.shard_map(
        fused_layer if fused else make(fs, tp),
        mesh=mesh,
        in_specs=placed,
        out_specs=P(("grp", "fs"), "tp"),
        check_vma=False,
    )
```

profile of v0, /device:TPU:3, one launch (start us, length us, event | category | flops | bytes accessed | tf_op | source)
XLA Modules:
  0.0 228.5 jit_solution(11967384390096021753)
XLA Ops:
  0.0 226.2 %fused_layer.1 = bf16[1024,512]{1,0:T(8,128)(2,1)} custom-call(bf16[1024,512]{1,0:T(8,128)(2,1)} %tokens.1, f32[512,256]{1,0:T(8,128)} %weight_u.1, f32[512,256]{1,0:T(8,128)} %weight_v.1, f32[256,512]{1,0:T(8,128)} %weight_out.1, f32[512,2048]{1,0:T(8,128)} %weight_up.1, f32[2048,512]{1,0:T(8,128)} %weight_down.1, f32[1,2048]{1,0:T(1,128)} %bitcast.8, ...), custom_call_target="tpu_custom_call" | custom-call | tf_op jit(solution)/shard_map/fused_layer/pallas_call | solution.py:677
  226.3 2.3 copy.18
where the time goes:
time: 229 us
  Pallas kernels  226 us (99%)
    pallas_call x1, Pallas kernels, fused_layer(): pl.pallas_call(fused_kernel, name='fused_layer', out_shape=jax.ShapeDtype...  226 us

commit v1 on v0

--- a/solution.py
+++ b/solution.py
@@ -230,16 +230,20 @@
     gain1, scale_u, scale_v, mix_gain, spatial_weight, spatial_bias,
     scale_out, scale_down, gain2, scale_up,
     result,
-    stage, g_both, g_out, g_up, g_down, tok, mid, normed, hidden,
-    act_v, gate_u, gated, stat, stat_rows, scales, terms, core_in, x_out, x_in,
-    load_sem, zs, zr, ys, yr, gs, gr, cs, cr, xs, xr, cs2, cr2, xs2, xr2,
-    sts, strv, scs, scr,
+    stage, g_both, g_out, g_up, g_down, tok, mid, mid_end, normed, hidden, hidden_end,
+    act_v, gate_u, gated, stat, stat_rows, scales, terms, core_in, core_end, x_out, x_in, x_end,
+    load_sem, zs, zr, ys, yr, zos, zor, gs, gr, cs, cr, xs, xr, cs2, cr2, xs2, xr2,
+    cs3, cr3, xs3, xr3, es, er, ps, pr, sts, strv, scs, scr,
 ):
     y, z, t = lax.axis_index("grp"), lax.axis_index("fs"), lax.axis_index("tp")
     other_y = 1 - y
     upper = z // 2
     planes = (z, 1 - z + 4 * upper, 2 - upper, 3 - 3 * upper)
     is_mid = (z == 1) | (z == 2)
+    is_end = jnp.logical_not(is_mid)
+    terms_end = tok
+    inner = (t == 1) | (t == 2)
+    outer = jnp.logical_not(inner)
     t1 = t + 1 - 2 * (t % 2)
     t2 = (t + 2) % 4
     t3 = (t1 + 2) % 4
@@ -305,12 +309,16 @@
         part = pl.ds(r * chunk, chunk)
         remote(buffer.at[block, part], buffer.at[block, part], gs.at[which, 2, r], gr.at[which, block, r], tp=t1).wait_recv()
 
-    def gather_relay(which, buffer, r):
+    def relay_copy(which, buffer, r):
+        part = pl.ds(r * chunk, chunk)
+        return remote(buffer.at[t2, part], buffer.at[t2, part], gs.at[which, 2, r], gr.at[which, t2, r], tp=t1)
+
+    def gather_relay(which, buffer, r, listed=True):
         gather_await(which, buffer, t2, r)
-        part = pl.ds(r * chunk, chunk)
-        copy = remote(buffer.at[t2, part], buffer.at[t2, part], gs.at[which, 2, r], gr.at[which, t2, r], tp=t1)
+        copy = relay_copy(which, buffer, r)
         copy.start()
-        sends.append(copy)
+        if listed:
+            sends.append(copy)
 
     def piece(w, p, h):
         if w == 0:
@@ -356,6 +364,29 @@
         for i in (1, 2, 3):
             arrive_y(w, i)
 
+    def other_half(w, p):
+        return remote(piece(w, p, other_y), piece(w, p, other_y), zos.at[w], zor.at[w], fs=planes[1])
+
+    def own_end(w, first):
+        @pl.when(is_end)
+        def _():
+            (z_copy(w, z, planes[1], 0) if first else other_half(w, z)).start()
+
+    def own_mid(w):
+        @pl.when(is_mid)
+        def _():
+            z_copy(w, z, planes[2], 1).start()
+
+    def pass_on(w, i):
+        @pl.when(is_mid)
+        def _():
+            p = planes[i]
+            z_copy(w, p, planes[1], 1 + i).wait_recv()
+            if i == 1:
+                z_copy(w, p, planes[2], 2).start()
+            else:
+                y_copy(w, i, y).start()
+
     for r in range(CHUNKS):
         gather_start(0, tok, tokens, r)
 
@@ -403,30 +434,32 @@
 
         cast_to(slot, fine, store)
 
-    own(1)
     cast_up(0, 2)
     load_down(0, 2).start()
-    gather_relay(0, tok, 0)
     cast_up(1, 3)
     load_down(1, 3).start()
     arrive(0, 1)
+    own(1)
     cast_up(2, 0)
     load_down(2, 0).start()
     cast_up(3, 1)
     load_down(3, 1).start()
-    arrive(1, 1)
+    own_end(2, True)
+    own_end(3, True)
+    own_mid(2)
+    arrive(0, 2)
+    gather_relay(0, tok, 0)
+    arrive(0, 3)
     gather_relay(0, tok, 1)
-    arrive(0, 2)
-    arrive(1, 2)
-    own(2)
     cast_down(0, 2)
     cast_down(1, 3)
-    gather_relay(0, tok, 2)
     cast_down(2, 0)
     cast_down(3, 1)
-    arrive(0, 3)
-    arrive(1, 3)
-    own(3)
+    gather_relay(0, tok, 2)
+    arrive(1, 1)
+    arrive(1, 2)
+    own_end(2, False)
+    own_end(3, False)
     load_tok.wait()
 
     def norm_rows(buffer, gain, first, count):
@@ -453,7 +486,7 @@
             gather_relay(0, tok, r)
         norm_chunk(0, tok, gain1, r)
 
-    arrive(2, 1)
+    own_mid(3)
     arrive_all_y(0)
 
     lane = lax.broadcasted_iota(jnp.int32, (chunk, 128), 1)
@@ -479,7 +512,7 @@
         copy.start()
         sends.append(copy)
     row_loop(0, rows, chunk, u_chunk)
-    arrive(2, 2)
+    arrive(1, 3)
     for k, u in ((1, t1), (2, t2), (3, t3)):
         stat_copy(k, u).wait_recv()
     totals = stat_rows[0] + stat_rows[1] + stat_rows[2] + stat_rows[3]
@@ -499,6 +532,8 @@
         gated[part, :] = (gate_u[part, :] * mixed).astype(jnp.bfloat16)
 
     row_loop(0, rows, BLOCK, mix_block)
+    pass_on(2, 1)
+    own_end(4, True)
     arrive_all_y(1)
     for i in (1, 2, 3):
         remote(scales.at[planes[i]], scales.at[planes[i]], scs.at[i - 1], scr.at[planes[i]], fs=planes[i]).wait_recv()
@@ -511,6 +546,11 @@
         part = pl.ds(r * chunk, chunk)
         return remote(x_out.at[part], x_in.at[part], send.at[r], recv.at[r], tp=t2)
 
+    def end_copy(r):
+        part = pl.ds(r * chunk, chunk)
+        return remote(mid.at[t, part], mid_end.at[t, part], gs.at[1, 0, r], gr.at[2, t, r], fs=planes[1])
+
+    pass_on(2, 2)
     mix_sends = []
     for r in range(CHUNKS):
         part = pl.ds(r * chunk, chunk)
@@ -536,8 +576,9 @@
         copy = x_copy(xs, xr, r)
         copy.start()
         mix_sends.append(copy)
-    own(4)
-    arrive(2, 3)
+    pass_on(3, 1)
+    pass_on(3, 2)
+    own_mid(4)
 
     for r in range(CHUNKS):
         x_copy(xs, xr, r).wait_recv()
@@ -548,118 +589,282 @@
             mid[t, part, :] = (tok[t, part, :].astype(jnp.float32) + total).astype(jnp.bfloat16)
 
         row_loop(r * chunk, chunk, STEP, residual_rows)
-        gather_start(1, mid, mid.at[t], r)
-        if r == 1:
-            arrive(3, 1)
-    arrive(3, 2)
-    for copy in mix_sends:
+
+        @pl.when(is_mid)
+        def _():
+            for copy in gather_copies(1, mid, mid.at[t], r):
+                copy.start()
+
+        @pl.when(is_end)
+        def _():
+            end_copy(r).start()
+
+        if r == 2:
+            pass_on(2, 3)
+
+    for copy in sends + mix_sends:
         copy.wait_send()
-    own(5)
-    for r in range(CHUNKS):
-        gather_relay(1, mid, r)
-        if r == 2:
-            arrive(3, 3)
-        if r > 0:
-            norm_chunk(1, mid, gain2, r - 1)
-    norm_chunk(1, mid, gain2, CHUNKS - 1)
 
     tile = min(hhalf, fine)
 
-    def up_half(h):
+    def up_half(target, h, first=0, count=rows):
         def body(part):
             for n in range(hhalf // tile):
                 cols = pl.ds(n * tile, tile)
                 place = rows_of(h * hhalf + n * tile, tile, 128)
                 value = matmul(normed[part, :], g_up[h, :, cols]) * scale_up[:, place]
                 value = jnp.maximum(value, 0.0)
-                hidden[part, place] = (value * value).astype(jnp.bfloat16)
-
-        row_loop(0, rows, chunk, body)
-
-    arrive(4, 1)
-    up_half(y)
-    arrive(4, 2)
-    arrive_all_y(2)
-    arrive_all_y(3)
-    up_half(other_y)
-    arrive(4, 3)
-
-    def chan_core(i, r):
+                target[part, place] = (value * value).astype(jnp.bfloat16)
+
+        row_loop(first, count, chunk, body)
+
+    sets = {
+        True: (hidden, terms, core_in, cs2, cr2),
+        False: (hidden_end, terms_end, core_end, cs3, cr3),
+    }
+
+    def chan_core(near, i, r):
+        _, out, into, send, recv = sets[near]
         j = planes[i]
         part = rows_of(r * chunk, chunk, chunk)
-        return remote(terms.at[j, part], core_in.at[j // 2, part], cs2.at[i, r], cr2.at[j // 2, r], tp=t1)
-
-    def down_piece(i):
+        return remote(out.at[j, part], into.at[j // 2, part], send.at[i, r], recv.at[j // 2, r], tp=t1)
+
+    def end_x_copy(slot, r):
+        part = pl.ds(r * chunk, chunk)
+        return remote(core_end.at[slot, part], x_end.at[part], xs3.at[r], xr3.at[r], tp=t2)
+
+    def pair_copy(slot, r):
+        part = pl.ds(r * chunk, chunk)
+        return remote(core_end.at[slot, part], core_in.at[slot, part], ps.at[r], pr.at[r], fs=planes[1])
+
+    def end_swap(slot, r):
+        part = pl.ds(r * chunk, chunk)
+        return remote(core_in.at[slot, part], x_in.at[part], xs2.at[r], xr2.at[r], tp=t2)
+
+    def back_copy(r):
+        part = pl.ds(r * chunk, chunk)
+        return remote(x_end.at[part], x_in.at[part], es.at[r], er.at[r], fs=planes[1])
+
+    def down_dots(near, i):
+        source, out = sets[near][:2]
         j = planes[i]
         mine = (j % 2) == (t % 2)
 
         def one(r, carry):
             part = rows_of(r * chunk, chunk, chunk)
-            product = matmul(hidden[part, :], g_down[j])
-            terms[j, part, :] = (product * scales[j, 1:2, :]).astype(jnp.bfloat16)
+            product = matmul(source[part, :], g_down[j])
+            out[j, part, :] = (product * scales[j, 1:2, :]).astype(jnp.bfloat16)
 
             @pl.when(jnp.logical_not(mine))
             def _():
-                chan_core(i, r).start()
+                chan_core(near, i, r).start()
 
             return carry
 
         lax.fori_loop(0, CHUNKS, one, 0)
 
-        @pl.when(mine)
+    def pair_up(near, i):
+        j = planes[i]
+        slot = j // 2
+
+        @pl.when((j % 2) == (t % 2))
         def _():
             for r in range(CHUNKS):
-                chan_core(i, r).wait_recv()
-
-                @pl.when(j != t)
-                def _():
-                    pair_out(j, j // 2, r)
-                    x_copy(xs2, xr2, r).start()
-
-    down_piece(0)
-    arrive(5, 1)
-    arrive_y(4, 1)
-    arrive(5, 2)
-    arrive_y(5, 1)
-    down_piece(1)
-    arrive(5, 3)
-    arrive_y(4, 2)
-    arrive_y(5, 2)
-    down_piece(2)
-    arrive_y(4, 3)
-    arrive_y(5, 3)
-    down_piece(3)
-
-    for r in range(CHUNKS):
-        x_copy(xs2, xr2, r).wait_recv()
-
-        def result_rows(part):
-            total = terms[t, part, :].astype(jnp.float32) + core_in[t // 2, part, :].astype(jnp.float32)
-            total = total + x_in[part, :].astype(jnp.float32)
-            result[part, :] = (mid[t, part, :].astype(jnp.float32) + total).astype(jnp.bfloat16)
-
-        row_loop(r * chunk, chunk, STEP, result_rows)
-
-    for copy in sends:
-        copy.wait_send()
-    for w in range(WAVES):
+                chan_core(near, i, r).wait_recv()
+                if near:
+                    @pl.when(j != t)
+                    def _():
+                        pair_out(j, slot, r)
+                        x_copy(xs2, xr2, r).start()
+                else:
+                    def body(part):
+                        both = tok[j, part, :].astype(jnp.float32) + core_end[slot, part, :].astype(jnp.float32)
+                        core_end[slot, part, :] = both.astype(jnp.bfloat16)
+
+                    if i in (0, 2):
+                        row_loop(r * chunk, chunk, STEP, body)
+                        pair_copy(slot, r).start()
+                    else:
+                        @pl.when(j != t)
+                        def _():
+                            row_loop(r * chunk, chunk, STEP, body)
+                            end_x_copy(slot, r).start()
+
+    def finish_end(i):
+        @pl.when(planes[i] == t)
+        def _():
+            for r in range(CHUNKS):
+                end_x_copy(t2 // 2, r).wait_recv()
+
+                def end_rows(part):
+                    total = tok[t, part, :].astype(jnp.float32) + core_end[t // 2, part, :].astype(jnp.float32)
+                    total = total + x_end[part, :].astype(jnp.float32)
+                    x_end[part, :] = (mid_end[t, part, :].astype(jnp.float32) + total).astype(jnp.bfloat16)
+
+                row_loop(r * chunk, chunk, STEP, end_rows)
+                back_copy(r).start()
+
+    @pl.when(is_mid)
+    def _():
+        own_mid(5)
+        gather_relay(1, mid, 0, False)
+        norm_chunk(1, mid, gain2, 0)
+        pass_on(3, 3)
+        gather_relay(1, mid, 1, False)
+        norm_chunk(1, mid, gain2, 1)
+        other_half(2, planes[1]).wait_recv()
+        other_half(3, planes[1]).wait_recv()
+        up_half(hidden, y, 0, 2 * chunk)
+        gather_relay(1, mid, 2, False)
+        norm_chunk(1, mid, gain2, 2)
+        up_half(hidden, y, 2 * chunk, chunk)
+        pass_on(4, 1)
+        for r in range(CHUNKS):
+            gather_await(2, mid_end, t, r)
+            for copy in gather_copies(2, mid_end, mid_end.at[t], r):
+                copy.start()
+        pass_on(4, 2)
+        pass_on(5, 2)
+        gather_relay(1, mid, 3, False)
+        norm_chunk(1, mid, gain2, 3)
+        up_half(hidden, y, 3 * chunk, chunk)
+        for w in (2, 3):
+            for i in (2, 3):
+                arrive_y(w, i)
+        up_half(hidden, other_y)
+        pass_on(4, 3)
+        pass_on(5, 1)
+
+        def end_chunk(r):
+            norm_chunk(2, mid_end, gain2, r)
+            for h in (0, 1):
+                up_half(hidden_end, h, r * chunk, chunk)
+
+        gather_relay(2, mid_end, 0, False)
+        gather_relay(2, mid_end, 1, False)
+        end_chunk(0)
+        gather_relay(2, mid_end, 2, False)
+        end_chunk(1)
+        down_dots(True, 0)
+        gather_relay(2, mid_end, 3, False)
+        end_chunk(2)
+        pair_up(True, 0)
+        pass_on(5, 3)
+        end_chunk(3)
+        for w in (4, 5):
+            arrive_y(w, 2)
+        down_dots(False, 0)
+        down_dots(False, 2)
+        pair_up(False, 0)
+        down_dots(True, 2)
+        for w in (4, 5):
+            other_half(w, planes[1]).wait_recv()
+        pair_up(False, 2)
+        down_dots(False, 1)
+        pair_up(True, 2)
+        for w in (4, 5):
+            arrive_y(w, 3)
+        down_dots(False, 3)
+        pair_up(False, 1)
+        down_dots(True, 1)
+        pair_up(False, 3)
+        down_dots(True, 3)
+        pair_up(True, 1)
+        pair_up(True, 3)
+        for i in (1, 3):
+            finish_end(i)
+        for r in range(CHUNKS):
+            x_copy(xs2, xr2, r).wait_recv()
+
+            def result_rows(part):
+                total = terms[t, part, :].astype(jnp.float32) + core_in[t // 2, part, :].astype(jnp.float32)
+                total = total + x_in[part, :].astype(jnp.float32)
+                result[part, :] = (mid[t, part, :].astype(jnp.float32) + total).astype(jnp.bfloat16)
+
+            row_loop(r * chunk, chunk, STEP, result_rows)
+
+    @pl.when(is_end)
+    def _():
+        z_copy(5, z, planes[1], 0).start()
+        z_copy(5, z, planes[1], 0).wait_send()
+        for w in (4, 5):
+            other_half(w, z).start()
+        near_slot = 1 - t % 2
+        for r in range(CHUNKS):
+            pair_copy(near_slot, r).wait_recv()
+
+            @pl.when(outer)
+            def _():
+                end_swap(near_slot, r).start()
+
+        @pl.when(inner)
+        def _():
+            for r in range(CHUNKS):
+                end_swap(near_slot, r).wait_recv()
+
+                def sum_rows(part):
+                    total = core_in[near_slot, part, :].astype(jnp.float32) + x_in[part, :].astype(jnp.float32)
+                    result[part, :] = (mid[t, part, :].astype(jnp.float32) + total).astype(jnp.bfloat16)
+
+                row_loop(r * chunk, chunk, STEP, sum_rows)
+
+        @pl.when(outer)
+        def _():
+            for r in range(CHUNKS):
+                back_copy(r).wait_recv()
+
+                def take_rows(part):
+                    result[part, :] = x_in[part, :]
+
+                row_loop(r * chunk, chunk, STEP, take_rows)
+                end_swap(near_slot, r).wait_send()
+
+    for w in (0, 1):
         z_copy(w, z, planes[1], 0).wait_send()
         for i in (1, 2, 3):
             y_copy(w, i, y).wait_send()
-    for r in range(CHUNKS):
-        x_copy(xs2, xr2, r).wait_send()
-    for i in range(4):
-        @pl.when((planes[i] % 2) != (t % 2))
-        def _():
-            for r in range(CHUNKS):
-                chan_core(i, r).wait_send()
+
+    @pl.when(is_end)
+    def _():
+        for w in range(2, WAVES):
+            if w < 5:
+                z_copy(w, z, planes[1], 0).wait_send()
+            other_half(w, z).wait_send()
+        for r in range(CHUNKS):
+            end_copy(r).wait_send()
 
     @pl.when(is_mid)
     def _():
-        for w in range(WAVES):
+        for w in (0, 1):
             z_copy(w, z, planes[2], 1).wait_send()
             for i in (1, 2, 3):
                 z_copy(w, planes[i], planes[1], 1 + i).wait_send()
+        for w in range(2, WAVES):
+            z_copy(w, z, planes[2], 1).wait_send()
+            z_copy(w, planes[1], planes[2], 2).wait_send()
+            for i in (2, 3):
+                y_copy(w, i, y).wait_send()
+        for r in range(CHUNKS):
+            x_copy(xs2, xr2, r).wait_send()
+            for which, buffer in ((1, mid), (2, mid_end)):
+                for copy in gather_copies(which, buffer, buffer.at[t], r):
+                    copy.wait_send()
+                relay_copy(which, buffer, r).wait_send()
+            pair_copy(1 - t % 2, r).wait_send()
+
+            @pl.when(inner)
+            def _():
+                end_x_copy(t2 // 2, r).wait_send()
+
+            @pl.when(outer)
+            def _():
+                back_copy(r).wait_send()
+        for i in range(4):
+            @pl.when((planes[i] % 2) != (t % 2))
+            def _():
+                for r in range(CHUNKS):
+                    chan_core(True, i, r).wait_send()
+                    chan_core(False, i, r).wait_send()
 
 
 def fused_layer(
@@ -688,7 +893,9 @@
             vmem((4, hid, fine), bf16),
             vmem((4, rows, fine), bf16),
             vmem((4, rows, fine), bf16),
+            vmem((4, rows, fine), bf16),
             vmem((rows, depth), bf16),
+            vmem((rows, hid), bf16),
             vmem((rows, hid), bf16),
             vmem((rows, width), f32),
             vmem((rows, width), f32),
@@ -698,13 +905,16 @@
             vmem((4, 2, fine), f32),
             vmem((4, rows, fine), bf16),
             vmem((2, rows, fine), bf16),
+            vmem((2, rows, fine), bf16),
+            vmem((rows, fine), bf16),
             vmem((rows, fine), bf16),
             vmem((rows, fine), bf16),
             dma(6),
-            dma(WAVES, 5), dma(WAVES, 4), dma(WAVES, 3), dma(WAVES, 4),
-            dma(2, 3, CHUNKS), dma(2, 4, CHUNKS),
+            dma(WAVES, 5), dma(WAVES, 4), dma(WAVES, 3), dma(WAVES, 4), dma(WAVES), dma(WAVES),
+            dma(3, 3, CHUNKS), dma(3, 4, CHUNKS),
             dma(2, CHUNKS), dma(2, CHUNKS), dma(CHUNKS), dma(CHUNKS),
             dma(4, CHUNKS), dma(2, CHUNKS), dma(CHUNKS), dma(CHUNKS),
+            dma(4, CHUNKS), dma(2, CHUNKS), dma(CHUNKS), dma(CHUNKS), dma(CHUNKS), dma(CHUNKS), dma(CHUNKS), dma(CHUNKS),
             dma(3), dma(4), dma(3), dma(4),
         ],
         compiler_params=pltpu.CompilerParams(

time: 229 us -> 177 us (0.77)
  the two profiles are of different devices: /device:TPU:3 before, /device:TPU:20 now
where the time goes in v1:
time: 177 us
  Pallas kernels  175 us (99%)
  local copies, waits for them, and re-layouts  2.26 us (1%)
    pallas_call x1, Pallas kernels, fused_layer(): pl.pallas_call(fused_kernel, name='fused_layer', out_shape=jax.ShapeDtype...  175 us

profile of v1, /device:TPU:20, one launch (start us, length us, event | category | flops | bytes accessed | tf_op | source)
XLA Modules:
  0.0 177.2 jit_solution(1869102549053793599)
XLA Ops:
  0.0 174.9 %fused_layer.1 = bf16[1024,512]{1,0:T(8,128)(2,1)} custom-call(bf16[1024,512]{1,0:T(8,128)(2,1)} %tokens.1, f32[512,256]{1,0:T(8,128)} %weight_u.1, f32[512,256]{1,0:T(8,128)} %weight_v.1, f32[256,512]{1,0:T(8,128)} %weight_out.1, f32[512,2048]{1,0:T(8,128)} %weight_up.1, f32[2048,512]{1,0:T(8,128)} %weight_down.1, f32[1,2048]{1,0:T(1,128)} %bitcast.8, ...), custom_call_target="tpu_custom_call" | custom-call | tf_op jit(solution)/shard_map/fused_layer/pallas_call | solution.py:882
  175.0 2.3 %copy.18 = bf16[1024,512]{1,0:T(8,128)(2,1)} copy(bf16[1024,512]{1,0:T(8,128)(2,1)} %fused_layer.1) | data formatting | bytes 2097152
